TPU v7x, 32 devices: a whole 2x2x4 slice. The times are simulated.
32 devices in a mesh: sp: 4 (over z), tp: 8 (over y, x, core).
Axes of the slice: x: 2, y: 2, z: 4, core: 2. Of those that a mesh axis runs over, the one named last changes fastest.
Arguments:
- stream: bfloat16 [1024, 4096], P('sp', 'tp'), may hold values from -80 to 80
- norm_gain: bfloat16 [3, 4096], replicated, may hold values from 0.099609375 to 1.8984375
- value_weight: bfloat16 [3, 2048, 4096], P(None, 'tp'), may hold values from -0.09375 to 0.09375
- gate_weight: bfloat16 [3, 2048, 4096], P(None, 'tp'), may hold values from -0.09375 to 0.09375
- kernel: float32 [3, 31, 2048], P(None, None, 'tp'), may hold values from -8 to 8
- kernel_bias: float32 [3, 2048], P(None, 'tp'), may hold values from -3 to 3
- chan_gain: float32 [3, 2048], P(None, 'tp'), may hold values from 0.1 to 1.9
- chan_shift: float32 [3, 2048], P(None, 'tp'), may hold values from -3 to 3
- out_weight: bfloat16 [3, 2048, 4096], P(None, None, 'tp'), may hold values from -0.125 to 0.125
Outputs:
- result: bfloat16 [1024, 4096], P('sp', 'tp')
All inputs are finite; a program needn't handle non-finite values.
Results may differ from a plain program's by a relative error of at most 0.012.
Values may be sent and summed in bfloat16 or wider, within the bound.
A program may use at most 64 MiB of HBM per device.

v0:
```python
import jax
import jax.numpy as jnp
from jax import lax
from jax.sharding import PartitionSpec as P

EPSILON = 1e-06


def passed_along(shard, axis, by):
    count = lax.axis_size(axis)
    pairs = [(i, i + by) for i in range(count) if 0 <= i + by < count]
    return lax.ppermute(shard, axis, pairs)


def against(left, right):
    return lax.dot_general(
        left, right, (((1,), (1,)), ((), ())), preferred_element_type=jnp.float32
    )


def on_device(
    stream,
    norm_gain,
    value_weight,
    gate_weight,
    kernel,
    kernel_bias,
    chan_gain,
    chan_shift,
    out_weight,
):
    layer_count = kernel.shape[0]
    reach_back = kernel.shape[1] - 1
    local_width = stream.shape[1]
    channels = kernel.shape[2] * lax.axis_size("tp")
    current = stream
    for layer_at in range(layer_count):
        gain_row = norm_gain[layer_at].astype(jnp.float32)
        value_matrix = value_weight[layer_at]
        gate_matrix = gate_weight[layer_at]
        row_count = current.shape[0]
        whole_rows = lax.all_gather(current, "tp", axis=1, tiled=True)
        whole_float = whole_rows.astype(jnp.float32)
        scale_row = lax.rsqrt(jnp.mean(whole_float * whole_float, axis=1, keepdims=True) + EPSILON)
        normed = (whole_float * scale_row * gain_row[None, :]).astype(jnp.bfloat16)
        value_part = against(normed, value_matrix)
        gate_part = against(normed, gate_matrix)
        gated_rows = (value_part * jax.nn.sigmoid(gate_part)).astype(jnp.bfloat16)
        earlier_taps = passed_along(gated_rows[row_count - reach_back :], "sp", 1)
        padded = jnp.concatenate([earlier_taps, gated_rows], axis=0)
        out_rows = padded.shape[0] - reach_back
        kernel_now = kernel[layer_at]
        convolved = jnp.broadcast_to(
            kernel_bias[layer_at][None, :], (out_rows, kernel_now.shape[1])
        )
        for tap_at in range(reach_back + 1):
            convolved = convolved + kernel_now[tap_at][None, :] * padded[
                tap_at : tap_at + out_rows
            ].astype(jnp.float32)
        totals = lax.psum(
            (jnp.sum(convolved, axis=1), jnp.sum(convolved * convolved, axis=1)), "tp"
        )
        centre = totals[0] / channels
        spread = totals[1] / channels - centre * centre
        normal_out = (convolved - centre[:, None]) * lax.rsqrt(spread + EPSILON)[
            :, None
        ] * chan_gain[layer_at][None, :] + chan_shift[layer_at][None, :]
        hidden = jax.nn.silu(normal_out).astype(jnp.bfloat16)
        out_matrix = out_weight[layer_at]

        def project_out(running, block_in, offset_at, out_matrix=out_matrix):
            return jnp.dot(block_in, out_matrix, preferred_element_type=jnp.float32)

        projected = project_out(
            jnp.zeros((out_rows, local_width), jnp.float32),
            lax.all_gather(hidden, "tp", axis=1, tiled=True),
            jnp.int32(0),
        )
        current = (current.astype(jnp.float32) + projected).astype(jnp.bfloat16)
    return current


def solution(mesh):
    return jax.shard_map(
        on_device,
        mesh=mesh,
        in_specs=(
            P("sp", "tp"),
            P(),
            P(None, "tp", None),
            P(None, "tp", None),
            P(None, None, "tp"),
            P(None, "tp"),
            P(None, "tp"),
            P(None, "tp"),
            P(None, None, "tp"),
        ),
        out_specs=P("sp", "tp"),
        check_vma=False,
    )
```

profile of v0, /device:TPU:0, one launch (start us, length us, event | category | flops | bytes accessed | tf_op | source)
XLA Modules:
  0.0 266.8 jit_solution(3278399664090631594)
XLA Ops:
  12.0 28.1 %all-gather.7.cloned.1.call-done = bf16[256,4096]{1,0:T(8,128)(2,1)} async-done(((bf16[256,512]{1,0:T(8,128)(2,1)}), bf16[256,4096]{1,0:T(8,128)(2,1)}) %all-gather.7.cloned.1.call-update) | async-done | bytes 2097168 | tf_op jit(solution)/shard_map/all_gather | solution.py:42
  40.1 2.1 fusion
  42.2 3.2 %fusion.96 = f32[256,256]{1,0:T(8,128)S(1)} fusion(bf16[3,256,4096]{2,1,0:T(8,128)(2,1)} %param.12, bf16[256,4096]{1,0:T(8,128)(2,1)} %all-gather.7.cloned.1.call-done, f32[4096]{0:T(1024)S(1)} %bitcast.187, f32[256]{0:T(256)S(1)} %add_rsqrt_fusion.5), kind=kOutput, calls=%fused_computation.149 | convolution fusion | flops 541261824 | bytes 4473856 | tf_op jit(solution)/shard_map/dot_general | solution.py:16
  45.4 2.5 fusion.105
  47.9 3.5 %collective-permute-start = (bf16[30,256]{1,0:T(8,128)(2,1)S(1)}, bf16[30,256]{1,0:T(8,128)(2,1)S(1)}, u32[]{:S(2)}, u32[]{:S(2)}) collective-permute-start(bf16[30,256]{1,0:T(8,128)(2,1)S(1)} %slice.1017), channel_id=1, source_target_pairs={{0,8},{8,16},{16,24},{1,9},{9,17},{17,25},{2,10},{10,18},{18,26},{... | collective-permute-start | bytes 46088 | tf_op jit(solution)/shard_map/ppermute | solution.py:12
  54.0 12.2 %all-reduce.2 = (f32[256]{0:T(256)S(1)}, f32[256]{0:T(256)S(1)}) all-reduce(f32[256]{0:T(256)S(1)} %get-tuple-element.10, f32[256]{0:T(256)S(1)} %get-tuple-element.9), channel_id=1, replica_groups=mesh['sp'=4,'tp'=8] {'tp'}, use_global_device_ids=true, to_apply=%region_4.0 | all-reduce | flops 512 | bytes 4096 | tf_op jit(solution)/shard_map/psum | solution.py:60
  67.2 24.1 %all-gather.9.cloned.1.call-done = bf16[256,2048]{1,0:T(8,128)(2,1)} async-done(((bf16[256,256]{1,0:T(8,128)(2,1)}), bf16[256,2048]{1,0:T(8,128)(2,1)}) %all-gather.9.cloned.1.call-update) | async-done | bytes 1048592 | tf_op jit(solution)/shard_map/all_gather | solution.py:76
  91.3 3.3 %fusion.51 = bf16[256,512]{1,0:T(8,128)(2,1)} fusion(bf16[256,2048]{1,0:T(8,128)(2,1)} %all-gather.9.cloned.1.call-done, bf16[3,2048,512]{2,1,0:T(8,128)(2,1)} %param.17, bf16[256,512]{1,0:T(8,128)(2,1)S(1)} %copy-done.3), kind=kOutput, calls=%fused_computation.134 | convolution fusion | flops 537264128 | bytes 3670016 | tf_op jit(solution)/shard_map/dot_general | solution.py:72
  94.7 28.2 %all-gather.11.cloned.1.call-done = bf16[256,4096]{1,0:T(8,128)(2,1)} async-done(((bf16[256,512]{1,0:T(8,128)(2,1)}), bf16[256,4096]{1,0:T(8,128)(2,1)}) %all-gather.11.cloned.1.call-update) | async-done | bytes 2097168 | tf_op jit(solution)/shard_map/all_gather | solution.py:42
  122.9 2.1 fusion.3
  125.0 3.2 %fusion.93 = f32[256,256]{1,0:T(8,128)S(1)} fusion(bf16[3,256,4096]{2,1,0:T(8,128)(2,1)} %param.12, bf16[256,4096]{1,0:T(8,128)(2,1)} %all-gather.11.cloned.1.call-done, f32[4096]{0:T(1024)S(1)} %bitcast.185, f32[256]{0:T(256)S(1)} %add_rsqrt_fusion.3), kind=kOutput, calls=%fused_computation.148 | convolution fusion | flops 541261824 | bytes 4473856 | tf_op jit(solution)/shard_map/dot_general | solution.py:16
  128.2 2.4 fusion.102
  130.7 3.4 %collective-permute-start.1 = (bf16[30,256]{1,0:T(8,128)(2,1)S(1)}, bf16[30,256]{1,0:T(8,128)(2,1)S(1)}, u32[]{:S(2)}, u32[]{:S(2)}) collective-permute-start(bf16[30,256]{1,0:T(8,128)(2,1)S(1)} %slice.1076), channel_id=1, source_target_pairs={{0,8},{8,16},{16,24},{1,9},{9,17},{17,25},{2,10},{10,18},{18,26},{... | collective-permute-start | bytes 46088 | tf_op jit(solution)/shard_map/ppermute | solution.py:12
  136.7 12.2 %all-reduce.1 = (f32[256]{0:T(256)S(1)}, f32[256]{0:T(256)S(1)}) all-reduce(f32[256]{0:T(256)S(1)} %get-tuple-element.8, f32[256]{0:T(256)S(1)} %get-tuple-element.7), channel_id=1, replica_groups=mesh['sp'=4,'tp'=8] {'tp'}, use_global_device_ids=true, to_apply=%region_9.10 | all-reduce | flops 512 | bytes 4096 | tf_op jit(solution)/shard_map/psum | solution.py:60
  149.8 24.1 %all-gather.13.cloned.1.call-done = bf16[256,2048]{1,0:T(8,128)(2,1)} async-done(((bf16[256,256]{1,0:T(8,128)(2,1)}), bf16[256,2048]{1,0:T(8,128)(2,1)}) %all-gather.13.cloned.1.call-update) | async-done | bytes 1048592 | tf_op jit(solution)/shard_map/all_gather | solution.py:76
  173.9 3.3 %fusion.48 = bf16[256,512]{1,0:T(8,128)(2,1)} fusion(bf16[256,2048]{1,0:T(8,128)(2,1)} %all-gather.13.cloned.1.call-done, bf16[3,2048,512]{2,1,0:T(8,128)(2,1)} %param.17, bf16[256,512]{1,0:T(8,128)(2,1)S(1)} %copy-done.4), kind=kOutput, calls=%fused_computation.133 | convolution fusion | flops 537264128 | bytes 3670016 | tf_op jit(solution)/shard_map/dot_general | solution.py:72
  177.3 28.2 %all-gather.15.cloned.1.call-done = bf16[256,4096]{1,0:T(8,128)(2,1)} async-done(((bf16[256,512]{1,0:T(8,128)(2,1)}), bf16[256,4096]{1,0:T(8,128)(2,1)}) %all-gather.15.cloned.1.call-update) | async-done | bytes 2097168 | tf_op jit(solution)/shard_map/all_gather | solution.py:42
  205.6 2.1 fusion.6
  207.7 3.2 %fusion.90 = f32[256,256]{1,0:T(8,128)S(1)} fusion(bf16[3,256,4096]{2,1,0:T(8,128)(2,1)} %param.12, bf16[256,4096]{1,0:T(8,128)(2,1)} %all-gather.15.cloned.1.call-done, f32[4096]{0:T(1024)S(1)} %bitcast.183, f32[256]{0:T(256)S(1)} %add_rsqrt_fusion.1), kind=kOutput, calls=%fused_computation.147 | convolution fusion | flops 541261824 | bytes 4473856 | tf_op jit(solution)/shard_map/dot_general | solution.py:16
  210.8 2.5 fusion.99
  213.3 3.4 %collective-permute-start.2 = (bf16[30,256]{1,0:T(8,128)(2,1)S(1)}, bf16[30,256]{1,0:T(8,128)(2,1)S(1)}, u32[]{:S(2)}, u32[]{:S(2)}) collective-permute-start(bf16[30,256]{1,0:T(8,128)(2,1)S(1)} %slice.1135), channel_id=1, source_target_pairs={{0,8},{8,16},{16,24},{1,9},{9,17},{17,25},{2,10},{10,18},{18,26},{... | collective-permute-start | bytes 46088 | tf_op jit(solution)/shard_map/ppermute | solution.py:12
  219.3 12.2 %all-reduce = (f32[256]{0:T(256)S(1)}, f32[256]{0:T(256)S(1)}) all-reduce(f32[256]{0:T(256)S(1)} %get-tuple-element.6, f32[256]{0:T(256)S(1)} %get-tuple-element.5), channel_id=1, replica_groups=mesh['sp'=4,'tp'=8] {'tp'}, use_global_device_ids=true, to_apply=%region_14.15 | all-reduce | flops 512 | bytes 4096 | tf_op jit(solution)/shard_map/psum | solution.py:60
  232.5 24.2 %all-gather.17.cloned.1.call-done = bf16[256,2048]{1,0:T(8,128)(2,1)} async-done(((bf16[256,256]{1,0:T(8,128)(2,1)}), bf16[256,2048]{1,0:T(8,128)(2,1)}) %all-gather.17.cloned.1.call-update) | async-done | bytes 1048592 | tf_op jit(solution)/shard_map/all_gather | solution.py:76
  256.6 3.3 %fusion.45 = bf16[256,512]{1,0:T(8,128)(2,1)} fusion(bf16[256,2048]{1,0:T(8,128)(2,1)} %all-gather.17.cloned.1.call-done, bf16[3,2048,512]{2,1,0:T(8,128)(2,1)} %param.17, bf16[256,512]{1,0:T(8,128)(2,1)S(1)} %copy-done.5), kind=kOutput, calls=%fused_computation.132 | convolution fusion | flops 537264128 | bytes 3670016 | tf_op jit(solution)/shard_map/dot_general | solution.py:72
  (55 shorter events, 16.2 us)
Async XLA Ops:
  6.5 33.5 %all-gather.7.cloned.1.call-start = ((), (), s32[]{:S(2)}) async-start(), calls=%async_computation | async-start | bytes 2359296 | tf_op jit(solution)/shard_map/all_gather | solution.py:42
  7.3 84.0 %all-gather.9.cloned.1.call-start = ((), (), s32[]{:S(2)}) async-start(), calls=%async_computation.1 | async-start | bytes 1179648 | tf_op jit(solution)/shard_map/all_gather | solution.py:76
  42.2 3.2 %copy-start = (bf16[256,4096]{1,0:T(8,128)(2,1)S(1)}, bf16[256,4096]{1,0:T(8,128)(2,1)}, u32[]{:S(2)}) copy-start(bf16[256,4096]{1,0:T(8,128)(2,1)} %all-gather.7.cloned.1.call-done) | copy-start | bytes 6291460
  45.3 6.0 %copy-start.7 = (f32[3,256]{1,0:T(4,128)S(1)}, f32[3,256]{1,0:T(4,128)}, u32[]{:S(2)}) copy-start(f32[3,256]{1,0:T(4,128)} %param.16) | copy-start | bytes 9220
  45.4 45.9 %copy-start.3 = (bf16[256,512]{1,0:T(8,128)(2,1)S(1)}, bf16[256,512]{1,0:T(8,128)(2,1)}, u32[]{:S(2)}) copy-start(bf16[256,512]{1,0:T(8,128)(2,1)} %param.9) | copy-start | bytes 786436
  47.8 46.9 %copy-start.6 = (f32[3,31,256]{2,1,0:T(8,128)S(1)}, f32[3,31,256]{2,1,0:T(8,128)}, u32[]{:S(2)}) copy-start(f32[3,31,256]{2,1,0:T(8,128)} %param.13) | copy-start | bytes 285700
  47.9 5.0 %collective-permute-start = (bf16[30,256]{1,0:T(8,128)(2,1)S(1)}, bf16[30,256]{1,0:T(8,128)(2,1)S(1)}, u32[]{:S(2)}, u32[]{:S(2)}) collective-permute-start(bf16[30,256]{1,0:T(8,128)(2,1)S(1)} %slice.1017), channel_id=1, source_target_pairs={{0,8},{8,16},{16,24},{1,9},{9,17},{17,25},{2,10},{10,18},{18,26},{... | collective-permute-start | bytes 46088 | tf_op jit(solution)/shard_map/ppermute | solution.py:12
  67.1 55.8 %all-gather.11.cloned.1.call-start = ((), (), s32[]{:S(2)}) async-start(), calls=%async_computation.2 | async-start | bytes 2359296 | tf_op jit(solution)/shard_map/all_gather | solution.py:42
  94.6 79.3 %all-gather.13.cloned.1.call-start = ((), (), s32[]{:S(2)}) async-start(), calls=%async_computation.3 | async-start | bytes 1179648 | tf_op jit(solution)/shard_map/all_gather | solution.py:76
  125.0 3.2 %copy-start.1 = (bf16[256,4096]{1,0:T(8,128)(2,1)S(1)}, bf16[256,4096]{1,0:T(8,128)(2,1)}, u32[]{:S(2)}) copy-start(bf16[256,4096]{1,0:T(8,128)(2,1)} %all-gather.11.cloned.1.call-done) | copy-start | bytes 6291460
  128.2 45.8 %copy-start.4 = (bf16[256,512]{1,0:T(8,128)(2,1)S(1)}, bf16[256,512]{1,0:T(8,128)(2,1)}, u32[]{:S(2)}) copy-start(bf16[256,512]{1,0:T(8,128)(2,1)} %fusion.51) | copy-start | bytes 786436
  130.7 4.8 %collective-permute-start.1 = (bf16[30,256]{1,0:T(8,128)(2,1)S(1)}, bf16[30,256]{1,0:T(8,128)(2,1)S(1)}, u32[]{:S(2)}, u32[]{:S(2)}) collective-permute-start(bf16[30,256]{1,0:T(8,128)(2,1)S(1)} %slice.1076), channel_id=1, source_target_pairs={{0,8},{8,16},{16,24},{1,9},{9,17},{17,25},{2,10},{10,18},{18,26},{... | collective-permute-start | bytes 46088 | tf_op jit(solution)/shard_map/ppermute | solution.py:12
  149.8 55.8 %all-gather.15.cloned.1.call-start = ((), (), s32[]{:S(2)}) async-start(), calls=%async_computation.4 | async-start | bytes 2359296 | tf_op jit(solution)/shard_map/all_gather | solution.py:42
  177.3 79.3 %all-gather.17.cloned.1.call-start = ((), (), s32[]{:S(2)}) async-start(), calls=%async_computation.5 | async-start | bytes 1179648 | tf_op jit(solution)/shard_map/all_gather | solution.py:76
  207.6 3.2 %copy-start.2 = (bf16[256,4096]{1,0:T(8,128)(2,1)S(1)}, bf16[256,4096]{1,0:T(8,128)(2,1)}, u32[]{:S(2)}) copy-start(bf16[256,4096]{1,0:T(8,128)(2,1)} %all-gather.15.cloned.1.call-done) | copy-start | bytes 6291460
  210.8 45.8 %copy-start.5 = (bf16[256,512]{1,0:T(8,128)(2,1)S(1)}, bf16[256,512]{1,0:T(8,128)(2,1)}, u32[]{:S(2)}) copy-start(bf16[256,512]{1,0:T(8,128)(2,1)} %fusion.48) | copy-start | bytes 786436
  213.3 4.8 %collective-permute-start.2 = (bf16[30,256]{1,0:T(8,128)(2,1)S(1)}, bf16[30,256]{1,0:T(8,128)(2,1)S(1)}, u32[]{:S(2)}, u32[]{:S(2)}) collective-permute-start(bf16[30,256]{1,0:T(8,128)(2,1)S(1)} %slice.1135), channel_id=1, source_target_pairs={{0,8},{8,16},{16,24},{1,9},{9,17},{17,25},{2,10},{10,18},{18,26},{... | collective-permute-start | bytes 46088 | tf_op jit(solution)/shard_map/ppermute | solution.py:12
Sparse Core Ops, SparseCore 0:
  9.2 30.8 all-gather.6
  67.3 23.9 all-gather.8
  94.8 28.0 all-gather.10
  149.9 23.9 all-gather.12
  177.4 28.0 all-gather.14
  232.6 23.9 all-gather.16
where the time goes:
time: 268 us; the launch traced here: 267 us
  waiting for transfers between devices  162 us (60%)
  blocking collectives  36.7 us (14%)
  matrix products  26.8 us (10%)
  between operations  13.7 us (5%)
  other arithmetic  13.3 us (5%)
  starting transfers between devices  10.5 us (4%)
  local copies, waits for them, and re-layouts  3.88 us (1%)
    all_gather x3, waiting for transfers between devices, on_device(): whole_rows = lax.all_gather(current, 'tp', axis=1, tiled=True)  84.5 us
    all_gather x3, waiting for transfers between devices, on_device(): lax.all_gather(hidden, 'tp', axis=1, tiled=True)  72.4 us
    psum x3, blocking collectives, on_device(): lax.psum((jnp.sum(convolved, axis=1), jnp.sum(convolved * convolved, axis...  36.7 us
    dot_general x6, matrix products, against(): lax.dot_general(left, right, (((1,), (1,)), ((), ())), preferred_element_...  16.8 us
    ppermute x3, starting transfers between devices, passed_along(): return lax.ppermute(shard, axis, pairs)  10.3 us
    dot_general x3, matrix products, project_out(): return jnp.dot(block_in, out_matrix, preferred_element_type=jnp.float32)  9.99 us
    reduce_sum x3, other arithmetic, on_device(): jnp.mean(whole_float * whole_float, axis=1, keepdims=True) + EPSILON  6.25 us
  transfers between devices with their start and end apart: 9, of which 9 were waited for; matrix products, arithmetic and copies ran while one was open for 2% of the time, Pallas kernels for 0%

commit v1 on v0

--- a/solution.py
+++ b/solution.py
@@ -4,6 +4,12 @@
 from jax.sharding import PartitionSpec as P
 
 EPSILON = 1e-06
+
+
+def all_parts(x, name, d):
+    terms = lax.all_gather(x, name, axis=0, tiled=False)
+    result = jnp.concatenate(terms, axis=d)
+    return result
 
 
 def passed_along(shard, axis, by):
@@ -73,7 +79,7 @@
 
         projected = project_out(
             jnp.zeros((out_rows, local_width), jnp.float32),
-            lax.all_gather(hidden, "tp", axis=1, tiled=True),
+            all_parts(hidden, "tp", 1),
             jnp.int32(0),
         )
         current = (current.astype(jnp.float32) + projected).astype(jnp.bfloat16)

time: 268 us -> 271 us (1.011)
  local copies, waits for them, and re-layouts: 3.88 us -> 8.3 us
    all_gather x0 -> x3, local copies, waits for them, and re-layouts: none -> 4.42 us  [all_parts(): terms = lax.all_gather(x, name, axis=0, tiled=False)]
where the time goes in v1:
time: 271 us; the launch traced here: 270 us
  waiting for transfers between devices  161 us (59%)
  blocking collectives  36.7 us (14%)
  matrix products  25.9 us (10%)
  between operations  13.8 us (5%)
  other arithmetic  13.3 us (5%)
  starting transfers between devices  10.5 us (4%)
  local copies, waits for them, and re-layouts  8.3 us (3%)
    all_gather x3, waiting for transfers between devices, on_device(): whole_rows = lax.all_gather(current, 'tp', axis=1, tiled=True)  84.5 us
    all_gather x3, waiting for transfers between devices, all_parts(): terms = lax.all_gather(x, name, axis=0, tiled=False)  72 us
    psum x3, blocking collectives, on_device(): lax.psum((jnp.sum(convolved, axis=1), jnp.sum(convolved * convolved, axis...  36.7 us
    dot_general x6, matrix products, against(): lax.dot_general(left, right, (((1,), (1,)), ((), ())), preferred_element_...  16.8 us
    ppermute x3, starting transfers between devices, passed_along(): return lax.ppermute(shard, axis, pairs)  10.3 us
    dot_general x3, matrix products, project_out(): return jnp.dot(block_in, out_matrix, preferred_element_type=jnp.float32)  9.08 us
    reduce_sum x3, other arithmetic, on_device(): jnp.mean(whole_float * whole_float, axis=1, keepdims=True) + EPSILON  6.25 us
  transfers between devices with their start and end apart: 9, of which 9 were waited for; matrix products, arithmetic and copies ran while one was open for 2% of the time, Pallas kernels for 0%

profile of v1, /device:TPU:0, one launch (start us, length us, event | category | flops | bytes accessed | tf_op | source)
XLA Modules:
  0.0 270.0 jit_solution(7608114176000158147)
XLA Ops:
  12.0 28.1 %all-gather.10.cloned.1.call-done = bf16[256,4096]{1,0:T(8,128)(2,1)} async-done(((bf16[256,512]{1,0:T(8,128)(2,1)}), bf16[256,4096]{1,0:T(8,128)(2,1)}) %all-gather.10.cloned.1.call-update) | async-done | bytes 2097168 | tf_op jit(solution)/shard_map/all_gather | solution.py:48
  40.1 2.1 fusion
  42.2 3.2 %fusion.96 = f32[256,256]{1,0:T(8,128)S(1)} fusion(bf16[3,256,4096]{2,1,0:T(8,128)(2,1)} %param.12, bf16[256,4096]{1,0:T(8,128)(2,1)} %all-gather.10.cloned.1.call-done, f32[4096]{0:T(1024)S(1)} %bitcast.205, f32[256]{0:T(256)S(1)} %add_rsqrt_fusion.5), kind=kOutput, calls=%fused_computation.149 | convolution fusion | flops 541261824 | bytes 4473856 | tf_op jit(solution)/shard_map/dot_general | solution.py:22
  45.4 2.5 fusion.105
  47.9 3.5 %collective-permute-start = (bf16[30,256]{1,0:T(8,128)(2,1)S(1)}, bf16[30,256]{1,0:T(8,128)(2,1)S(1)}, u32[]{:S(2)}, u32[]{:S(2)}) collective-permute-start(bf16[30,256]{1,0:T(8,128)(2,1)S(1)} %slice.1017), channel_id=1, source_target_pairs={{0,8},{8,16},{16,24},{1,9},{9,17},{17,25},{2,10},{10,18},{18,26},{... | collective-permute-start | bytes 46088 | tf_op jit(solution)/shard_map/ppermute | solution.py:18
  54.0 12.2 %all-reduce.2 = (f32[256]{0:T(256)S(1)}, f32[256]{0:T(256)S(1)}) all-reduce(f32[256]{0:T(256)S(1)} %get-tuple-element.10, f32[256]{0:T(256)S(1)} %get-tuple-element.9), channel_id=1, replica_groups=mesh['sp'=4,'tp'=8] {'tp'}, use_global_device_ids=true, to_apply=%region_4.0 | all-reduce | flops 512 | bytes 4096 | tf_op jit(solution)/shard_map/psum | solution.py:66
  67.2 24.0 %all-gather.16.cloned.1.call-done = bf16[2048,256]{1,0:T(8,128)(2,1)} async-done(((bf16[256,256]{1,0:T(8,128)(2,1)}), bf16[2048,256]{1,0:T(8,128)(2,1)}) %all-gather.16.cloned.1.call-update) | async-done | bytes 1048592 | tf_op jit(solution)/shard_map/all_gather | solution.py:10
  92.7 3.0 %fusion.51 = bf16[256,512]{1,0:T(8,128)(2,1)} fusion(bf16[256,2048]{0,1:T(8,128)(2,1)S(1)} %bitcast.200, bf16[3,2048,512]{2,1,0:T(8,128)(2,1)} %param.17, bf16[256,512]{1,0:T(8,128)(2,1)S(1)} %copy-done.3), kind=kOutput, calls=%fused_computation.134 | convolution fusion | flops 537264128 | bytes 3670016 | tf_op jit(solution)/shard_map/dot_general | solution.py:78
  95.8 28.2 %all-gather.12.cloned.1.call-done = bf16[256,4096]{1,0:T(8,128)(2,1)} async-done(((bf16[256,512]{1,0:T(8,128)(2,1)}), bf16[256,4096]{1,0:T(8,128)(2,1)}) %all-gather.12.cloned.1.call-update) | async-done | bytes 2097168 | tf_op jit(solution)/shard_map/all_gather | solution.py:48
  124.0 2.1 fusion.3
  126.1 3.2 %fusion.93 = f32[256,256]{1,0:T(8,128)S(1)} fusion(bf16[3,256,4096]{2,1,0:T(8,128)(2,1)} %param.12, bf16[256,4096]{1,0:T(8,128)(2,1)} %all-gather.12.cloned.1.call-done, f32[4096]{0:T(1024)S(1)} %bitcast.203, f32[256]{0:T(256)S(1)} %add_rsqrt_fusion.3), kind=kOutput, calls=%fused_computation.148 | convolution fusion | flops 541261824 | bytes 4473856 | tf_op jit(solution)/shard_map/dot_general | solution.py:22
  129.3 2.4 fusion.102
  131.7 3.4 %collective-permute-start.1 = (bf16[30,256]{1,0:T(8,128)(2,1)S(1)}, bf16[30,256]{1,0:T(8,128)(2,1)S(1)}, u32[]{:S(2)}, u32[]{:S(2)}) collective-permute-start(bf16[30,256]{1,0:T(8,128)(2,1)S(1)} %slice.1076), channel_id=1, source_target_pairs={{0,8},{8,16},{16,24},{1,9},{9,17},{17,25},{2,10},{10,18},{18,26},{... | collective-permute-start | bytes 46088 | tf_op jit(solution)/shard_map/ppermute | solution.py:18
  137.8 12.2 %all-reduce.1 = (f32[256]{0:T(256)S(1)}, f32[256]{0:T(256)S(1)}) all-reduce(f32[256]{0:T(256)S(1)} %get-tuple-element.8, f32[256]{0:T(256)S(1)} %get-tuple-element.7), channel_id=1, replica_groups=mesh['sp'=4,'tp'=8] {'tp'}, use_global_device_ids=true, to_apply=%region_9.10 | all-reduce | flops 512 | bytes 4096 | tf_op jit(solution)/shard_map/psum | solution.py:66
  150.9 24.0 %all-gather.18.cloned.1.call-done = bf16[2048,256]{1,0:T(8,128)(2,1)} async-done(((bf16[256,256]{1,0:T(8,128)(2,1)}), bf16[2048,256]{1,0:T(8,128)(2,1)}) %all-gather.18.cloned.1.call-update) | async-done | bytes 1048592 | tf_op jit(solution)/shard_map/all_gather | solution.py:10
  176.4 3.0 %fusion.48 = bf16[256,512]{1,0:T(8,128)(2,1)} fusion(bf16[256,2048]{0,1:T(8,128)(2,1)S(1)} %bitcast.198, bf16[3,2048,512]{2,1,0:T(8,128)(2,1)} %param.17, bf16[256,512]{1,0:T(8,128)(2,1)S(1)} %copy-done.4), kind=kOutput, calls=%fused_computation.133 | convolution fusion | flops 537264128 | bytes 3670016 | tf_op jit(solution)/shard_map/dot_general | solution.py:78
  179.5 28.2 %all-gather.14.cloned.1.call-done = bf16[256,4096]{1,0:T(8,128)(2,1)} async-done(((bf16[256,512]{1,0:T(8,128)(2,1)}), bf16[256,4096]{1,0:T(8,128)(2,1)}) %all-gather.14.cloned.1.call-update) | async-done | bytes 2097168 | tf_op jit(solution)/shard_map/all_gather | solution.py:48
  207.7 2.1 fusion.6
  209.8 3.2 %fusion.90 = f32[256,256]{1,0:T(8,128)S(1)} fusion(bf16[3,256,4096]{2,1,0:T(8,128)(2,1)} %param.12, bf16[256,4096]{1,0:T(8,128)(2,1)} %all-gather.14.cloned.1.call-done, f32[4096]{0:T(1024)S(1)} %bitcast.201, f32[256]{0:T(256)S(1)} %add_rsqrt_fusion.1), kind=kOutput, calls=%fused_computation.147 | convolution fusion | flops 541261824 | bytes 4473856 | tf_op jit(solution)/shard_map/dot_general | solution.py:22
  213.0 2.5 fusion.99
  215.5 3.4 %collective-permute-start.2 = (bf16[30,256]{1,0:T(8,128)(2,1)S(1)}, bf16[30,256]{1,0:T(8,128)(2,1)S(1)}, u32[]{:S(2)}, u32[]{:S(2)}) collective-permute-start(bf16[30,256]{1,0:T(8,128)(2,1)S(1)} %slice.1135), channel_id=1, source_target_pairs={{0,8},{8,16},{16,24},{1,9},{9,17},{17,25},{2,10},{10,18},{18,26},{... | collective-permute-start | bytes 46088 | tf_op jit(solution)/shard_map/ppermute | solution.py:18
  221.5 12.2 %all-reduce = (f32[256]{0:T(256)S(1)}, f32[256]{0:T(256)S(1)}) all-reduce(f32[256]{0:T(256)S(1)} %get-tuple-element.6, f32[256]{0:T(256)S(1)} %get-tuple-element.5), channel_id=1, replica_groups=mesh['sp'=4,'tp'=8] {'tp'}, use_global_device_ids=true, to_apply=%region_14.15 | all-reduce | flops 512 | bytes 4096 | tf_op jit(solution)/shard_map/psum | solution.py:66
  234.6 24.0 %all-gather.20.cloned.1.call-done = bf16[2048,256]{1,0:T(8,128)(2,1)} async-done(((bf16[256,256]{1,0:T(8,128)(2,1)}), bf16[2048,256]{1,0:T(8,128)(2,1)}) %all-gather.20.cloned.1.call-update) | async-done | bytes 1048592 | tf_op jit(solution)/shard_map/all_gather | solution.py:10
  260.1 3.0 %fusion.45 = bf16[256,512]{1,0:T(8,128)(2,1)} fusion(bf16[256,2048]{0,1:T(8,128)(2,1)S(1)} %bitcast.199, bf16[3,2048,512]{2,1,0:T(8,128)(2,1)} %param.17, bf16[256,512]{1,0:T(8,128)(2,1)S(1)} %copy-done.5), kind=kOutput, calls=%fused_computation.132 | convolution fusion | flops 537264128 | bytes 3670016 | tf_op jit(solution)/shard_map/dot_general | solution.py:78
  (58 shorter events, 20.6 us)
Async XLA Ops:
  6.5 33.5 %all-gather.10.cloned.1.call-start = ((), (), s32[]{:S(2)}) async-start(), calls=%async_computation | async-start | bytes 2359296 | tf_op jit(solution)/shard_map/all_gather | solution.py:48
  7.3 83.9 %all-gather.16.cloned.1.call-start = ((), (), s32[]{:S(2)}) async-start(), calls=%async_computation.3 | async-start | bytes 1179648 | tf_op jit(solution)/shard_map/all_gather | solution.py:10
  42.2 3.2 %copy-start = (bf16[256,4096]{1,0:T(8,128)(2,1)S(1)}, bf16[256,4096]{1,0:T(8,128)(2,1)}, u32[]{:S(2)}) copy-start(bf16[256,4096]{1,0:T(8,128)(2,1)} %all-gather.10.cloned.1.call-done) | copy-start | bytes 6291460
  45.3 6.0 %copy-start.7 = (f32[3,256]{1,0:T(4,128)S(1)}, f32[3,256]{1,0:T(4,128)}, u32[]{:S(2)}) copy-start(f32[3,256]{1,0:T(4,128)} %param.16) | copy-start | bytes 9220
  45.4 47.3 %copy-start.3 = (bf16[256,512]{1,0:T(8,128)(2,1)S(1)}, bf16[256,512]{1,0:T(8,128)(2,1)}, u32[]{:S(2)}) copy-start(bf16[256,512]{1,0:T(8,128)(2,1)} %param.9) | copy-start | bytes 786436
  47.8 47.9 %copy-start.6 = (f32[3,31,256]{2,1,0:T(8,128)S(1)}, f32[3,31,256]{2,1,0:T(8,128)}, u32[]{:S(2)}) copy-start(f32[3,31,256]{2,1,0:T(8,128)} %param.13) | copy-start | bytes 285700
  47.9 5.0 %collective-permute-start = (bf16[30,256]{1,0:T(8,128)(2,1)S(1)}, bf16[30,256]{1,0:T(8,128)(2,1)S(1)}, u32[]{:S(2)}, u32[]{:S(2)}) collective-permute-start(bf16[30,256]{1,0:T(8,128)(2,1)S(1)} %slice.1017), channel_id=1, source_target_pairs={{0,8},{8,16},{16,24},{1,9},{9,17},{17,25},{2,10},{10,18},{18,26},{... | collective-permute-start | bytes 46088 | tf_op jit(solution)/shard_map/ppermute | solution.py:18
  67.1 56.8 %all-gather.12.cloned.1.call-start = ((), (), s32[]{:S(2)}) async-start(), calls=%async_computation.1 | async-start | bytes 2359296 | tf_op jit(solution)/shard_map/all_gather | solution.py:48
  95.7 79.2 %all-gather.18.cloned.1.call-start = ((), (), s32[]{:S(2)}) async-start(), calls=%async_computation.4 | async-start | bytes 1179648 | tf_op jit(solution)/shard_map/all_gather | solution.py:10
  126.1 3.2 %copy-start.1 = (bf16[256,4096]{1,0:T(8,128)(2,1)S(1)}, bf16[256,4096]{1,0:T(8,128)(2,1)}, u32[]{:S(2)}) copy-start(bf16[256,4096]{1,0:T(8,128)(2,1)} %all-gather.12.cloned.1.call-done) | copy-start | bytes 6291460
  129.3 47.1 %copy-start.4 = (bf16[256,512]{1,0:T(8,128)(2,1)S(1)}, bf16[256,512]{1,0:T(8,128)(2,1)}, u32[]{:S(2)}) copy-start(bf16[256,512]{1,0:T(8,128)(2,1)} %fusion.51) | copy-start | bytes 786436
  131.7 4.8 %collective-permute-start.1 = (bf16[30,256]{1,0:T(8,128)(2,1)S(1)}, bf16[30,256]{1,0:T(8,128)(2,1)S(1)}, u32[]{:S(2)}, u32[]{:S(2)}) collective-permute-start(bf16[30,256]{1,0:T(8,128)(2,1)S(1)} %slice.1076), channel_id=1, source_target_pairs={{0,8},{8,16},{16,24},{1,9},{9,17},{17,25},{2,10},{10,18},{18,26},{... | collective-permute-start | bytes 46088 | tf_op jit(solution)/shard_map/ppermute | solution.py:18
  150.9 56.8 %all-gather.14.cloned.1.call-start = ((), (), s32[]{:S(2)}) async-start(), calls=%async_computation.2 | async-start | bytes 2359296 | tf_op jit(solution)/shard_map/all_gather | solution.py:48
  179.4 79.2 %all-gather.20.cloned.1.call-start = ((), (), s32[]{:S(2)}) async-start(), calls=%async_computation.5 | async-start | bytes 1179648 | tf_op jit(solution)/shard_map/all_gather | solution.py:10
  209.8 3.2 %copy-start.2 = (bf16[256,4096]{1,0:T(8,128)(2,1)S(1)}, bf16[256,4096]{1,0:T(8,128)(2,1)}, u32[]{:S(2)}) copy-start(bf16[256,4096]{1,0:T(8,128)(2,1)} %all-gather.14.cloned.1.call-done) | copy-start | bytes 6291460
  213.0 47.1 %copy-start.5 = (bf16[256,512]{1,0:T(8,128)(2,1)S(1)}, bf16[256,512]{1,0:T(8,128)(2,1)}, u32[]{:S(2)}) copy-start(bf16[256,512]{1,0:T(8,128)(2,1)} %fusion.48) | copy-start | bytes 786436
  215.5 4.8 %collective-permute-start.2 = (bf16[30,256]{1,0:T(8,128)(2,1)S(1)}, bf16[30,256]{1,0:T(8,128)(2,1)S(1)}, u32[]{:S(2)}, u32[]{:S(2)}) collective-permute-start(bf16[30,256]{1,0:T(8,128)(2,1)S(1)} %slice.1135), channel_id=1, source_target_pairs={{0,8},{8,16},{16,24},{1,9},{9,17},{17,25},{2,10},{10,18},{18,26},{... | collective-permute-start | bytes 46088 | tf_op jit(solution)/shard_map/ppermute | solution.py:18
Sparse Core Ops, SparseCore 0:
  9.2 30.8 all-gather.9
  67.3 23.8 all-gather.15
  95.8 28.0 all-gather.11
  151.0 23.8 all-gather.17
  179.6 28.0 all-gather.13
  234.7 23.8 all-gather.19
